TPU v7x, 256 devices: a whole 4x4x8 slice. The times are simulated.
256 devices in a mesh: sp: 64 (over z, y, core), tp: 4 (over x).
Axes of the slice: x: 4, y: 4, z: 8, core: 2. Of those that a mesh axis runs over, the one named last changes fastest.
Arguments:
- out_grad: bfloat16 [12288, 2048], P('sp'), may hold values from -16 to 16
- routes: int32 [12288, 2], P('sp'), may hold values from 0 to 63, all different within a row; in each aligned block of 192 rows (0 to 191, 192 to 383, ...) at most 12 rows name the same one
- route_weight: float32 [12288, 2], P('sp'), may hold values from 0.3 to 1.5
- expert_rows: bfloat16 [64, 64, 12, 2048], P(None, 'sp'), may hold values from -6 to 6
- gate_weight: bfloat16 [64, 2048, 1024], P('sp', None, 'tp'), may hold values from -0.125 to 0.125
- up_weight: bfloat16 [64, 2048, 1024], P('sp', None, 'tp'), may hold values from -0.125 to 0.125
- down_weight: bfloat16 [64, 1024, 2048], P('sp', 'tp'), may hold values from -0.1875 to 0.1875
- conv_input: bfloat16 [12288, 1024], P('sp', 'tp'), may hold values from -6 to 6
- out_gate: bfloat16 [12288, 1024], P('sp', 'tp'), may hold values from -6 to 6
- in_gate: bfloat16 [12288, 1024], P('sp', 'tp'), may hold values from -6 to 6
- taps: float32 [3, 1024], P(None, 'tp'), may hold values from -3 to 3
- out_weight: bfloat16 [2048, 1024], P(None, 'tp'), may hold values from -0.1875 to 0.1875
Outputs:
- gate_grad: bfloat16 [64, 2048, 1024], P('sp', None, 'tp')
- up_grad: bfloat16 [64, 2048, 1024], P('sp', None, 'tp')
- down_grad: bfloat16 [64, 1024, 2048], P('sp', 'tp')
- mid_grad: bfloat16 [12288, 2048], P('sp', 'tp')
- out_weight_grad: float32 [2048, 1024], P('sp', 'tp')
- input_grad: bfloat16 [12288, 1024], P('sp', 'tp')
- out_gate_grad: bfloat16 [12288, 1024], P('sp', 'tp')
- in_gate_grad: bfloat16 [12288, 1024], P('sp', 'tp')
Inputs may be any that keep to these rules, and one draw needn't show every extreme that they name: `routes`: each token names 2 different experts; within each aligned block of 192 tokens no expert is named by more than 12 tokens, a bound that some block reaches.
All inputs are finite; a program needn't handle non-finite values.
Results may differ from a plain program's by a relative error of at most 0.014.
Values may be sent and summed in bfloat16 or wider, within the bound.
No kernel may reach another device: no remote copies, remote signals or barrier semaphores. Data moves between devices by JAX's collectives and lax.ppermute only.
A program may use at most 64 MiB of HBM per device.

v0:
```python
import jax
import jax.numpy as jnp
from jax import lax
from jax.sharding import PartitionSpec as P


def split_up(shard, dim, peers):
    shape = shard.shape
    pieces = shard.reshape(*shape[:dim], peers, shape[dim] // peers, *shape[dim + 1 :])
    return jnp.moveaxis(pieces, dim, 0)


def sum_at_owner(shard, axis, dim):
    peers = lax.axis_size(axis)
    pieces = lax.all_to_all(split_up(shard, dim, peers), axis, 0, 0, tiled=True)
    return jnp.sum(pieces.astype(jnp.float32), axis=0)


def passed_along(shard, axis, by):
    peers = lax.axis_size(axis)
    pairs = [(i, i + by) for i in range(peers) if 0 <= i + by < peers]
    return lax.ppermute(shard, axis, pairs)


def on_device(
    out_grad,
    routes,
    route_weight,
    expert_rows,
    gate_weight,
    up_weight,
    down_weight,
    conv_input,
    out_gate,
    in_gate,
    taps,
    out_weight,
):
    groups = lax.axis_size("tp")
    member = lax.axis_index("tp")
    sources = lax.axis_size("sp")
    tok_rows, width = out_grad.shape
    top = routes.shape[1]
    local = gate_weight.shape[0]
    experts = local * sources
    slots = expert_rows.shape[2]
    share = width // groups
    flat = routes.reshape(-1)
    onehot = (flat[:, None] == jnp.arange(experts, dtype=jnp.int32)[None, :]).astype(jnp.int32)
    place = jnp.sum((jnp.cumsum(onehot, axis=0) - onehot) * onehot, axis=1)
    target = flat * slots + place
    slot_grad = (route_weight[:, :, None] * out_grad[:, None, :].astype(jnp.float32)).astype(
        jnp.bfloat16
    )
    outgoing = (
        jnp.zeros((experts * slots, width), jnp.bfloat16)
        .at[target]
        .set(slot_grad.reshape(-1, width))
    )
    outgoing = outgoing.reshape(sources, local, slots, width)
    portion = slots // groups
    piece = lax.dynamic_slice_in_dim(outgoing, member * portion, portion, 2)
    arrived = lax.all_to_all(piece, "sp", split_axis=0, concat_axis=0, tiled=True)
    grads = lax.all_gather(arrived, "tp", axis=2, tiled=True)
    gate = jnp.einsum(
        "secd,edf->secf", expert_rows, gate_weight, preferred_element_type=jnp.float32
    )
    up = jnp.einsum("secd,edf->secf", expert_rows, up_weight, preferred_element_type=jnp.float32)
    sig = jax.nn.sigmoid(gate)
    act = (gate * sig * up).astype(jnp.bfloat16)
    act_grad = jnp.einsum("secd,efd->secf", grads, down_weight, preferred_element_type=jnp.float32)
    up_part = (act_grad * gate * sig).astype(jnp.bfloat16)
    gate_part = (act_grad * up * sig * (1.0 + gate * (1.0 - sig))).astype(jnp.bfloat16)
    down_grad = jnp.einsum("secf,secd->efd", act, grads, preferred_element_type=jnp.float32).astype(
        jnp.bfloat16
    )
    gate_grad = jnp.einsum(
        "secd,secf->edf", expert_rows, gate_part, preferred_element_type=jnp.float32
    ).astype(jnp.bfloat16)
    up_grad = jnp.einsum(
        "secd,secf->edf", expert_rows, up_part, preferred_element_type=jnp.float32
    ).astype(jnp.bfloat16)
    row_part = jnp.einsum(
        "secf,edf->secd", gate_part, gate_weight, preferred_element_type=jnp.float32
    )
    row_part = row_part + jnp.einsum(
        "secf,edf->secd", up_part, up_weight, preferred_element_type=jnp.float32
    )
    summed = sum_at_owner(row_part.astype(jnp.bfloat16), "tp", 3)
    returned = lax.all_to_all(
        summed.astype(jnp.bfloat16), "sp", split_axis=0, concat_axis=0, tiled=True
    )
    returned = returned.reshape(experts * slots, share)
    picked = (
        jnp.take(returned, target, axis=0)
        .astype(jnp.float32)
        .reshape(tok_rows, top, share)
        .sum(axis=1)
    )
    own_cols = lax.dynamic_slice_in_dim(out_grad, member * share, share, 1).astype(jnp.float32)
    mid_grad = (own_cols + picked).astype(jnp.bfloat16)
    mid_whole = lax.all_gather(mid_grad, "tp", axis=1, tiled=True)
    reach = taps.shape[0] - 1
    rims = jnp.stack([in_gate[tok_rows - reach :], conv_input[tok_rows - reach :]])
    prior = passed_along(rims, "sp", 1)
    mixed = in_gate.astype(jnp.float32) * conv_input.astype(jnp.float32)
    prior_mixed = prior[0].astype(jnp.float32) * prior[1].astype(jnp.float32)
    extended = jnp.concatenate([prior_mixed, mixed], axis=0)
    conv = jnp.zeros_like(mixed)
    for tap in range(reach + 1):
        conv = conv + taps[tap][None, :] * extended[reach - tap : reach - tap + tok_rows]
    gated = (out_gate.astype(jnp.float32) * conv).astype(jnp.bfloat16)
    out_weight_grad = sum_at_owner(
        lax.dot_general(
            mid_whole, gated, (((0,), (0,)), ((), ())), preferred_element_type=jnp.float32
        ).astype(jnp.bfloat16),
        "sp",
        0,
    )
    gated_grad = jnp.dot(mid_whole, out_weight, preferred_element_type=jnp.float32)
    out_gate_grad = (gated_grad * conv).astype(jnp.bfloat16)
    conv_grad = gated_grad * out_gate.astype(jnp.float32)
    later = passed_along(conv_grad[:reach], "sp", -1)
    following = jnp.concatenate([conv_grad, later], axis=0)
    mixed_grad = jnp.zeros_like(conv_grad)
    for tap in range(reach + 1):
        mixed_grad = mixed_grad + taps[tap][None, :] * following[tap : tap + tok_rows]
    input_grad = (mixed_grad * in_gate.astype(jnp.float32)).astype(jnp.bfloat16)
    in_gate_grad = (mixed_grad * conv_input.astype(jnp.float32)).astype(jnp.bfloat16)
    return (
        gate_grad,
        up_grad,
        down_grad,
        mid_grad,
        out_weight_grad,
        input_grad,
        out_gate_grad,
        in_gate_grad,
    )


def solution(mesh):
    in_specs = (
        P("sp", None),
        P("sp", None),
        P("sp", None),
        P(None, "sp", None, None),
        P("sp", None, "tp"),
        P("sp", None, "tp"),
        P("sp", "tp", None),
        P("sp", "tp"),
        P("sp", "tp"),
        P("sp", "tp"),
        P(None, "tp"),
        P(None, "tp"),
    )
    out_specs = (
        P("sp", None, "tp"),
        P("sp", None, "tp"),
        P("sp", "tp", None),
        P("sp", "tp"),
        P("sp", "tp"),
        P("sp", "tp"),
        P("sp", "tp"),
        P("sp", "tp"),
    )
    return jax.shard_map(
        on_device, mesh=mesh, in_specs=in_specs, out_specs=out_specs, check_vma=False
    )
```

profile of v0, /device:TPU:1, one launch (start us, length us, event | category | flops | bytes accessed | tf_op | source)
XLA Modules:
  0.0 281.8 jit_solution(15357142444350941405)
XLA Ops:
  7.2 0.8 broadcast_multiply_fusion
  8.1 0.9 copy.44
  9.5 0.9 reduce-window.6
  10.4 0.2 slice_reduce_fusion
  10.7 4.4 %mul.148 = f32[192,2,2048]{2,1,0:T(2,128)} broadcast(bf16[192,2048]{1,0:T(8,128)(2,1)} %param.12), dimensions={0,2} | broadcast | bytes 3932160 | tf_op jit(solution)/shard_map/mul | solution.py:52
  15.1 5.3 %mul.149 = f32[384,2048]{1,0:T(8,128)} reshape(f32[192,2,2048]{2,1,0:T(2,128)} %mul.148) | data formatting | bytes 6291456 | tf_op jit(solution)/shard_map/mul | solution.py:52
  20.8 6.4 %scatter_custom_fusion = bf16[768,2048]{1,0:T(8,128)(2,1)} fusion(s32[384]{0:T(512)S(1)} %fusion.80, f32[384,2048]{1,0:T(8,128)} %mul.149, f32[384]{0:T(512)S(1)} %mul.146, bf16[]{:T(256)} %constant.12.clone.1), kind=kCustom, calls=%fused_computation.28 | custom fusion | flops 1572864 | bytes 6293506 | tf_op jit(solution)/shard_map/scatter | solution.py:58
  27.2 6.1 %reshape.145 = bf16[64,1,12,2048]{3,2,0,1:T(8,128)(2,1)} reshape(bf16[768,2048]{1,0:T(8,128)(2,1)} %scatter_custom_fusion) | data formatting | bytes 6291456 | tf_op jit(solution)/shard_map/reshape | solution.py:60
  33.2 3.0 %dynamic-slice_bitcast_fusion = bf16[64,1,3,2048]{3,2,1,0:T(4,128)(2,1)S(1)} fusion(bf16[64,1,12,2048]{3,2,0,1:T(8,128)(2,1)} %reshape.145, s32[]{:T(128)S(6)} %select_n.30), kind=kLoop, calls=%fused_computation.40 | loop fusion | bytes 1572868 | tf_op jit(solution)/shard_map/dynamic_slice | solution.py:62
  36.3 41.1 %all_to_all.20 = bf16[64,1,3,2048]{3,2,1,0:T(4,128)(2,1)S(1)} all-to-all(bf16[64,1,3,2048]{3,2,1,0:T(4,128)(2,1)S(1)} %dynamic-slice_bitcast_fusion), channel_id=1, replica_groups=mesh['sp'=64,'tp'=4] {'sp'}, dimensions={0} | all-to-all | bytes 1572864 | tf_op jit(solution)/shard_map/all_to_all | solution.py:63
  77.4 1.5 copy.49
  78.9 3.2 %fusion.48 = f32[64,1,12,256]{3,0,2,1:T(8,128)} fusion(bf16[64,1,12,2048]{3,0,2,1:T(8,128)(2,1)S(1)} %copy-done, bf16[1,2048,256]{2,1,0:T(8,128)(2,1)} %param.16), kind=kOutput, calls=%fused_computation.33 | convolution fusion | flops 805306368 | bytes 4980736 | tf_op jit(solution)/shard_map/secd,edf->secf/dot_general | solution.py:65
  82.1 1.9 fusion.45
  84.0 33.8 %all-gather.2.cloned.1.call-done = bf16[64,1,12,2048]{3,0,1,2:T(8,128)(2,1)} async-done(((bf16[64,1,3,2048]{3,0,1,2:T(8,128)(2,1)}), bf16[64,1,12,2048]{3,0,1,2:T(8,128)(2,1)}) %all-gather.2.cloned.1.call-update) | async-done | bytes 3145744 | tf_op jit(solution)/shard_map/all_gather | solution.py:64
  117.8 3.9 %multiply_convert_fusion.3 = (bf16[64,1,12,256]{3,0,2,1:T(8,128)(2,1)S(1)}, bf16[64,1,12,256]{3,0,2,1:T(8,128)(2,1)S(1)}) fusion(f32[64,1,12,256]{3,0,2,1:T(8,128)} %fusion.48, f32[64,1,12,256]{3,0,2,1:T(8,128)} %fusion.45, bf16[1,256,2048]{2,1,0:T(8,128)(2,1)} %param.18, bf16[64,1,12,2048]{3,0,1,2:T(8,128)(2,1)} %all-gather.2.cloned.1.call-done), kind=kOutput, calls=%fused_computation.43 | convolution fusion | flops 807862272 | bytes 6553600 | tf_op jit(solution)/shard_map/secd,efd->secf/dot_general | solution.py:71
  121.7 1.0 fusion.51
  122.7 0.4 copy-done.3
  123.2 1.0 add_convert_fusion
  124.2 0.4 copy.62
  124.6 39.9 %all_to_all.21 = bf16[4,64,1,12,512]{4,1,3,2,0:T(8,128)(2,1)} all-to-all(bf16[4,64,1,12,512]{4,1,3,2,0:T(8,128)(2,1)S(1)} %bitcast.161), channel_id=1, replica_groups=mesh['sp'=64,'tp'=4] {'tp'}, dimensions={0} | all-to-all | bytes 6291456 | tf_op jit(solution)/shard_map/all_to_all | solution.py:15
  164.5 3.5 %reduce_sum.48 = bf16[64,12,512]{2,0,1:T(8,128)(2,1)} reduce(bf16[4,64,1,12,512]{4,1,3,2,0:T(8,128)(2,1)} %all_to_all.21, bf16[]{:T(256)} %constant.12.clone.1), dimensions={0,2}, to_apply=%region_4.5 | reduce | flops 1179648 | bytes 3932162 | tf_op jit(solution)/shard_map/reduce_sum | solution.py:16
  168.1 2.5 copy.54
  170.6 12.1 %all-to-all-start.2 = ((bf16[64,1,12,512]{3,2,1,0:T(8,128)(2,1)}), bf16[64,1,12,512]{3,2,1,0:T(8,128)(2,1)}, u32[]{:S(2)}, u32[]{:S(2)}) async-start(bf16[64,1,12,512]{3,2,1,0:T(8,128)(2,1)} %copy.54), calls=%async_computation.2 | async-start | bytes 2097152 | tf_op jit(solution)/shard_map/all_to_all | solution.py:90
  182.8 3.5 %collective-permute-start = (bf16[2,2,256]{2,1,0:T(2,128)(2,1)S(1)}, bf16[2,2,256]{2,1,0:T(2,128)(2,1)S(1)}, u32[]{:S(2)}, u32[]{:S(2)}) collective-permute-start(bf16[2,2,256]{2,1,0:T(2,128)(2,1)S(1)} %pad_maximum_fusion.2), channel_id=1, source_target_pairs={{0,4},{4,8},{8,12},{12,16},{16,20},{20,24},{24,28},{28,32},{32,36}... | collective-permute-start | bytes 6152 | tf_op jit(solution)/shard_map/ppermute | solution.py:22
  186.6 0.7 convert_multiply_fusion.1
  187.3 0.7 copy.51
  188.1 0.6 multiply_bitcast_fusion
  188.6 22.2 %all-to-all-done.2 = bf16[64,1,12,512]{3,2,1,0:T(8,128)(2,1)} async-done(((bf16[64,1,12,512]{3,2,1,0:T(8,128)(2,1)}), bf16[64,1,12,512]{3,2,1,0:T(8,128)(2,1)}, u32[]{:S(2)}, u32[]{:S(2)}) %all-to-all-start.2) | async-done | bytes 786464 | tf_op jit(solution)/shard_map/all_to_all | solution.py:90
  210.8 2.1 reshape.155
  212.9 3.3 %gather_fusion = bf16[384,512]{1,0:T(8,128)(2,1)S(1)} fusion(bf16[768,512]{1,0:T(8,128)(2,1)} %reshape.155, s32[1024]{0:T(1024)S(1)} %pad_clamp_fusion), kind=kCustom, calls=%fused_computation | custom fusion | bytes 787968 | tf_op jit(solution)/shard_map/jit(_take)/gather | solution.py:95
  216.2 0.9 gather.7
  217.1 2.2 convert_reduce_fusion.1
  219.3 1.0 add_convert_fusion.1
  220.3 11.0 %all_gather.7 = bf16[192,2048]{1,0:T(8,128)(2,1)S(1)} all-gather(bf16[192,512]{1,0:T(8,128)(2,1)S(1)} %add_convert_fusion.1), channel_id=1, replica_groups=mesh['sp'=64,'tp'=4] {'tp'}, dimensions={1}, use_global_device_ids=true | all-gather | bytes 983040 | tf_op jit(solution)/shard_map/all_gather | solution.py:102
  231.3 2.5 multiply_convert_fusion.6
  233.7 1.5 convolution_convert_fusion
  235.2 9.6 %all-to-all-start.3 = ((bf16[64,32,256]{2,1,0:T(8,128)(2,1)}), bf16[64,32,256]{2,1,0:T(8,128)(2,1)}, u32[]{:S(2)}, u32[]{:S(2)}) async-start(bf16[64,32,256]{2,1,0:T(8,128)(2,1)} %bitcast.163), calls=%async_computation.3 | async-start | bytes 2097152 | tf_op jit(solution)/shard_map/all_to_all | solution.py:15
  244.9 3.1 %fusion.33 = bf16[1,2048,256]{1,2,0:T(8,128)(2,1)} fusion(bf16[64,1,12,2048]{3,0,2,1:T(8,128)(2,1)S(1)} %copy-done, bf16[64,1,12,256]{3,0,2,1:T(8,128)(2,1)} %copy-done.12), kind=kOutput, calls=%fused_computation.25 | convolution fusion | flops 805830656 | bytes 4587520 | tf_op jit(solution)/shard_map/secd,secf->edf/dot_general | solution.py:77
  248.0 2.0 fusion.30
  250.1 0.6 slice.66
  250.6 2.4 collective-permute-start.1
  253.1 2.0 fusion.36
  255.1 2.3 copy.55
  257.4 2.3 copy.56
  259.6 0.7 fusion.72
  260.3 0.7 fusion.71
  261.0 11.9 %all-to-all-done.3 = bf16[64,32,256]{2,1,0:T(8,128)(2,1)} async-done(((bf16[64,32,256]{2,1,0:T(8,128)(2,1)}), bf16[64,32,256]{2,1,0:T(8,128)(2,1)}, u32[]{:S(2)}, u32[]{:S(2)}) %all-to-all-start.3) | async-done | bytes 1048608 | tf_op jit(solution)/shard_map/all_to_all | solution.py:15
  272.9 2.0 convert_reduce_fusion
  (60 shorter events, 1.4 us)
Async XLA Ops:
  7.2 71.7 %copy-start = (bf16[64,1,12,2048]{3,0,2,1:T(8,128)(2,1)S(1)}, bf16[64,1,12,2048]{3,0,2,1:T(8,128)(2,1)}, u32[]{:S(2)}) copy-start(bf16[64,1,12,2048]{3,0,2,1:T(8,128)(2,1)} %param.15) | copy-start | bytes 9437188
  7.2 110.6 %all-gather.2.cloned.1.call-start = ((), (), s32[]{:S(2)}) async-start(), calls=%async_computation.4 | async-start | bytes 3932160 | tf_op jit(solution)/shard_map/all_gather | solution.py:64
  15.1 5.3 %copy-start.16 = (f32[192,2]{0,1:T(2,128)S(1)}, f32[192,2]{0,1:T(2,128)}, u32[]{:S(2)}) copy-start(f32[192,2]{0,1:T(2,128)} %param.14) | copy-start | bytes 4612
  78.9 3.2 %copy-start.2 = (bf16[1,2048,256]{2,1,0:T(8,128)(2,1)S(1)}, bf16[1,2048,256]{2,1,0:T(8,128)(2,1)}, u32[]{:S(2)}) copy-start(bf16[1,2048,256]{2,1,0:T(8,128)(2,1)} %param.17) | copy-start | bytes 3145732
  117.8 3.9 %copy-start.1 = (bf16[1,2048,256]{2,1,0:T(8,128)(2,1)S(1)}, bf16[1,2048,256]{2,1,0:T(8,128)(2,1)}, u32[]{:S(2)}) copy-start(bf16[1,2048,256]{2,1,0:T(8,128)(2,1)} %param.16) | copy-start | bytes 3145732
  121.7 1.1 copy-start.12
  121.7 1.1 copy-start.10
  121.7 1.5 copy-start.3
  164.5 18.2 %copy-start.5 = (bf16[192,256]{1,0:T(8,128)(2,1)S(1)}, bf16[192,256]{1,0:T(8,128)(2,1)}, u32[]{:S(2)}) copy-start(bf16[192,256]{1,0:T(8,128)(2,1)} %param.19) | copy-start | bytes 294916
  164.5 18.2 %copy-start.7 = (bf16[192,256]{1,0:T(8,128)(2,1)S(1)}, bf16[192,256]{1,0:T(8,128)(2,1)}, u32[]{:S(2)}) copy-start(bf16[192,256]{1,0:T(8,128)(2,1)} %param.21) | copy-start | bytes 294916
  164.5 22.0 %copy-start.13 = (s32[192,2]{0,1:T(2,128)S(1)}, s32[192,2]{0,1:T(2,128)}, u32[]{:S(2)}) copy-start(s32[192,2]{0,1:T(2,128)} %param.13) | copy-start | bytes 4612
  164.5 22.1 %copy-start.15 = (f32[3,256]{1,0:T(4,128)S(1)}, f32[3,256]{1,0:T(4,128)}, u32[]{:S(2)}) copy-start(f32[3,256]{1,0:T(4,128)} %param.22) | copy-start | bytes 9220
  170.6 40.2 %all-to-all-start.2 = ((bf16[64,1,12,512]{3,2,1,0:T(8,128)(2,1)}), bf16[64,1,12,512]{3,2,1,0:T(8,128)(2,1)}, u32[]{:S(2)}, u32[]{:S(2)}) async-start(bf16[64,1,12,512]{3,2,1,0:T(8,128)(2,1)} %copy.54), calls=%async_computation.2 | async-start | bytes 2097152 | tf_op jit(solution)/shard_map/all_to_all | solution.py:90
  182.8 5.3 %collective-permute-start = (bf16[2,2,256]{2,1,0:T(2,128)(2,1)S(1)}, bf16[2,2,256]{2,1,0:T(2,128)(2,1)S(1)}, u32[]{:S(2)}, u32[]{:S(2)}) collective-permute-start(bf16[2,2,256]{2,1,0:T(2,128)(2,1)S(1)} %pad_maximum_fusion.2), channel_id=1, source_target_pairs={{0,4},{4,8},{8,12},{12,16},{16,20},{20,24},{24,28},{28,32},{32,36}... | collective-permute-start | bytes 6152 | tf_op jit(solution)/shard_map/ppermute | solution.py:22
  216.2 15.1 %copy-start.14 = (f32[2,256]{1,0:T(2,128)S(1)}, f32[2,256]{1,0:T(2,128)}, u32[]{:S(2)}) copy-start(f32[2,256]{1,0:T(2,128)} %multiply_bitcast_fusion) | copy-start | bytes 6148
  217.1 16.6 %copy-start.9 = (bf16[192,256]{1,0:T(8,128)(2,1)S(1)}, bf16[192,256]{1,0:T(8,128)(2,1)}, u32[]{:S(2)}) copy-start(bf16[192,256]{1,0:T(8,128)(2,1)} %param.20) | copy-start | bytes 294916
  220.3 14.9 %copy-start.4 = (bf16[192,512]{1,0:T(8,128)(2,1)}, bf16[192,512]{1,0:T(8,128)(2,1)S(1)}, u32[]{:S(2)}) copy-start(bf16[192,512]{1,0:T(8,128)(2,1)S(1)} %add_convert_fusion.1) | copy-start | bytes 589828
  235.2 37.7 %all-to-all-start.3 = ((bf16[64,32,256]{2,1,0:T(8,128)(2,1)}), bf16[64,32,256]{2,1,0:T(8,128)(2,1)}, u32[]{:S(2)}, u32[]{:S(2)}) async-start(bf16[64,32,256]{2,1,0:T(8,128)(2,1)} %bitcast.163), calls=%async_computation.3 | async-start | bytes 2097152 | tf_op jit(solution)/shard_map/all_to_all | solution.py:15
  244.9 3.2 %copy-start.17 = (bf16[64,1,12,2048]{3,0,1,2:T(8,128)(2,1)S(1)}, bf16[64,1,12,2048]{3,0,1,2:T(8,128)(2,1)}, u32[]{:S(2)}) copy-start(bf16[64,1,12,2048]{3,0,1,2:T(8,128)(2,1)} %all-gather.2.cloned.1.call-done) | copy-start | bytes 9437188
  244.9 3.1 %copy-start.18 = (f32[64,1,12,256]{3,0,2,1:T(8,128)S(1)}, f32[64,1,12,256]{3,0,2,1:T(8,128)}, u32[]{:S(2)}) copy-start(f32[64,1,12,256]{3,0,2,1:T(8,128)} %fusion.48) | copy-start | bytes 2359300
  244.9 3.1 %copy-start.19 = (f32[64,1,12,256]{3,0,2,1:T(8,128)S(1)}, f32[64,1,12,256]{3,0,2,1:T(8,128)}, u32[]{:S(2)}) copy-start(f32[64,1,12,256]{3,0,2,1:T(8,128)} %fusion.45) | copy-start | bytes 2359300
  248.0 5.1 %copy-start.11 = (bf16[64,1,12,256]{3,0,2,1:T(8,128)(2,1)S(1)}, bf16[64,1,12,256]{3,0,2,1:T(8,128)(2,1)}, u32[]{:S(2)}) copy-start(bf16[64,1,12,256]{3,0,2,1:T(8,128)(2,1)} %copy-done.10) | copy-start | bytes 1179652
  250.6 9.0 %collective-permute-start.1 = (f32[2,256]{1,0:T(2,128)}, f32[2,256]{1,0:T(2,128)S(1)}, u32[]{:S(2)}, u32[]{:S(2)}) collective-permute-start(f32[2,256]{1,0:T(2,128)} %slice.66), channel_id=1, source_target_pairs={{4,0},{8,4},{12,8},{16,12},{20,16},{24,20},{28,24},{32,28},{36,32}... | collective-permute-start | bytes 6152 | tf_op jit(solution)/shard_map/ppermute | solution.py:22
  255.1 4.6 %copy-start.6 = (bf16[192,256]{1,0:T(8,128)(2,1)S(1)}, bf16[192,256]{1,0:T(8,128)(2,1)}, u32[]{:S(2)}) copy-start(bf16[192,256]{1,0:T(8,128)(2,1)} %param.19) | copy-start | bytes 294916
  255.1 5.3 %copy-start.8 = (bf16[192,256]{1,0:T(8,128)(2,1)S(1)}, bf16[192,256]{1,0:T(8,128)(2,1)}, u32[]{:S(2)}) copy-start(bf16[192,256]{1,0:T(8,128)(2,1)} %param.21) | copy-start | bytes 294916
Sparse Core Ops, SparseCore 0:
  79.0 38.7 all-gather.1
where the time goes:
time: 283 us; the launch traced here: 282 us
  blocking collectives  92 us (33%)
  waiting for transfers between devices  67.9 us (24%)
  local copies, waits for them, and re-layouts  37.9 us (13%)
  starting transfers between devices  27.8 us (10%)
  matrix products  22 us (8%)
  other arithmetic  19.7 us (7%)
  between operations  14.4 us (5%)
    all_to_all x1, blocking collectives, on_device(): lax.all_to_all(piece, 'sp', split_axis=0, concat_axis=0, tiled=True)  41.1 us
    all_to_all x1, blocking collectives, sum_at_owner(): pieces = lax.all_to_all(split_up(shard, dim, peers), axis, 0, 0, tiled=True)  39.9 us
    all_gather x1, waiting for transfers between devices, on_device(): grads = lax.all_gather(arrived, 'tp', axis=2, tiled=True)  33.8 us
    all_to_all x1, waiting for transfers between devices, on_device(): lax.all_to_all(summed.astype(jnp.bfloat16), 'sp', split_axis=0, concat_ax...  22.2 us
    all_to_all x1, starting transfers between devices, on_device(): lax.all_to_all(summed.astype(jnp.bfloat16), 'sp', split_axis=0, concat_ax...  12.1 us
    all_to_all x1, waiting for transfers between devices, sum_at_owner(): pieces = lax.all_to_all(split_up(shard, dim, peers), axis, 0, 0, tiled=True)  11.9 us
    all_gather x1, blocking collectives, on_device(): mid_whole = lax.all_gather(mid_grad, 'tp', axis=1, tiled=True)  11 us
    mul x3, local copies, waits for them, and re-layouts, on_device(): route_weight[:, :, None] * out_grad[:, None, :].astype(jnp.float32)  9.84 us
  transfers between devices with their start and end apart: 5, of which 3 were waited for; matrix products, arithmetic and copies ran while one was open for 7% of the time, Pallas kernels for 0%

commit v1 on v0

--- a/solution.py
+++ b/solution.py
@@ -61,7 +61,11 @@
     portion = slots // groups
     piece = lax.dynamic_slice_in_dim(outgoing, member * portion, portion, 2)
     arrived = lax.all_to_all(piece, "sp", split_axis=0, concat_axis=0, tiled=True)
-    grads = lax.all_gather(arrived, "tp", axis=2, tiled=True)
+    devices = lax.axis_size("tp")
+    repeats = [devices if d == 2 else 1 for d in range(arrived.ndim)]
+    grads = lax.all_to_all(
+        jnp.tile(arrived, repeats), "tp", split_axis=2, concat_axis=2, tiled=True
+    )
     gate = jnp.einsum(
         "secd,edf->secf", expert_rows, gate_weight, preferred_element_type=jnp.float32
     )

time: 283 us -> 269 us (0.951)
  between operations: 14.4 us -> 0.98 us
  waiting for transfers between devices: 67.9 us -> 63.5 us
    all_gather x1 -> x0, waiting for transfers between devices: 33.8 us -> none  [on_device(): grads = lax.all_gather(arrived, 'tp', axis=2, tiled=True)]
    all_to_all x0 -> x1, waiting for transfers between devices: none -> 31.3 us  [on_device(): lax.all_to_all(jnp.tile(arrived, repeats), 'tp', split_axis=2, concat_axi...]
    all_to_all x0 -> x1, starting transfers between devices: none -> 4.83 us  [on_device(): lax.all_to_all(jnp.tile(arrived, repeats), 'tp', split_axis=2, concat_axi...]
    unnamed x44 -> x42, local copies, waits for them, and re-layouts: 6.07 us -> 6.11 us
  transfers between devices with their start and end apart: 5 -> 5, of which waited for: 3 -> 3; matrix products, arithmetic and copies ran while one was open for 7% -> 9% of each run, Pallas kernels for 0% -> 0%
where the time goes in v1:
time: 269 us; the launch traced here: 268 us
  blocking collectives  90.8 us (34%)
  waiting for transfers between devices  63.5 us (24%)
  local copies, waits for them, and re-layouts  39.2 us (15%)
  starting transfers between devices  29.9 us (11%)
  matrix products  24 us (9%)
  other arithmetic  19.8 us (7%)
    all_to_all x1, blocking collectives, on_device(): lax.all_to_all(piece, 'sp', split_axis=0, concat_axis=0, tiled=True)  41.1 us
    all_to_all x1, blocking collectives, sum_at_owner(): pieces = lax.all_to_all(split_up(shard, dim, peers), axis, 0, 0, tiled=True)  38.7 us
    all_to_all x1, waiting for transfers between devices, on_device(): lax.all_to_all(jnp.tile(arrived, repeats), 'tp', split_axis=2, concat_axi...  31.3 us
    all_to_all x1, waiting for transfers between devices, on_device(): lax.all_to_all(summed.astype(jnp.bfloat16), 'sp', split_axis=0, concat_ax...  22.2 us
    all_gather x1, blocking collectives, on_device(): mid_whole = lax.all_gather(mid_grad, 'tp', axis=1, tiled=True)  11 us
    all_to_all x1, waiting for transfers between devices, sum_at_owner(): pieces = lax.all_to_all(split_up(shard, dim, peers), axis, 0, 0, tiled=True)  10 us
    mul x3, local copies, waits for them, and re-layouts, on_device(): route_weight[:, :, None] * out_grad[:, None, :].astype(jnp.float32)  9.85 us
    all_to_all x1, starting transfers between devices, sum_at_owner(): pieces = lax.all_to_all(split_up(shard, dim, peers), axis, 0, 0, tiled=True)  9.48 us
  transfers between devices with their start and end apart: 5, of which 3 were waited for; matrix products, arithmetic and copies ran while one was open for 9% of the time, Pallas kernels for 0%

profile of v1, /device:TPU:1, one launch (start us, length us, event | category | flops | bytes accessed | tf_op | source)
XLA Modules:
  0.0 268.0 jit_solution(3812791939933531819)
XLA Ops:
  0.6 0.8 broadcast_multiply_fusion
  1.5 0.9 copy.44
  3.0 0.9 reduce-window.6
  4.2 4.4 %mul.148 = f32[192,2,2048]{2,1,0:T(2,128)} broadcast(bf16[192,2048]{1,0:T(8,128)(2,1)} %param.12), dimensions={0,2} | broadcast | bytes 3932160 | tf_op jit(solution)/shard_map/mul | solution.py:52
  8.6 5.3 %mul.149 = f32[384,2048]{1,0:T(8,128)} reshape(f32[192,2,2048]{2,1,0:T(2,128)} %mul.148) | data formatting | bytes 6291456 | tf_op jit(solution)/shard_map/mul | solution.py:52
  14.3 6.4 %scatter_custom_fusion = bf16[768,2048]{1,0:T(8,128)(2,1)} fusion(s32[384]{0:T(512)S(1)} %fusion.80, f32[384,2048]{1,0:T(8,128)} %mul.149, f32[384]{0:T(512)S(1)} %mul.146, bf16[]{:T(256)} %constant.12.clone.1), kind=kCustom, calls=%fused_computation.28 | custom fusion | flops 1572864 | bytes 6293506 | tf_op jit(solution)/shard_map/scatter | solution.py:58
  20.7 6.1 %reshape.151 = bf16[64,1,12,2048]{3,2,0,1:T(8,128)(2,1)} reshape(bf16[768,2048]{1,0:T(8,128)(2,1)} %scatter_custom_fusion) | data formatting | bytes 6291456 | tf_op jit(solution)/shard_map/reshape | solution.py:60
  26.7 3.0 %dynamic-slice_bitcast_fusion = bf16[64,1,3,2048]{3,2,1,0:T(4,128)(2,1)S(1)} fusion(bf16[64,1,12,2048]{3,2,0,1:T(8,128)(2,1)} %reshape.151, s32[]{:T(128)S(6)} %select_n.30), kind=kLoop, calls=%fused_computation.40 | loop fusion | bytes 1572868 | tf_op jit(solution)/shard_map/dynamic_slice | solution.py:62
  29.8 41.1 %all_to_all.25 = bf16[64,1,3,2048]{3,2,1,0:T(4,128)(2,1)S(1)} all-to-all(bf16[64,1,3,2048]{3,2,1,0:T(4,128)(2,1)S(1)} %dynamic-slice_bitcast_fusion), channel_id=1, replica_groups=mesh['sp'=64,'tp'=4] {'sp'}, dimensions={0} | all-to-all | bytes 1572864 | tf_op jit(solution)/shard_map/all_to_all | solution.py:63
  70.9 0.6 copy.49
  71.4 2.1 tile.12
  73.5 4.8 %all-to-all-start.1 = ((bf16[64,1,12,2048]{3,0,1,2:T(8,128)(2,1)}), bf16[64,1,12,2048]{3,0,1,2:T(8,128)(2,1)}, u32[]{:S(2)}, u32[]{:S(2)}) async-start(bf16[64,1,12,2048]{3,0,1,2:T(8,128)(2,1)} %bitcast.164), calls=%async_computation.1 | async-start | bytes 6291456 | tf_op jit(solution)/shard_map/all_to_all | solution.py:66
  78.4 3.2 %fusion.48 = f32[64,1,12,256]{3,0,2,1:T(8,128)} fusion(bf16[64,1,12,2048]{3,0,2,1:T(8,128)(2,1)S(1)} %copy-done, bf16[1,2048,256]{2,1,0:T(8,128)(2,1)} %param.16), kind=kOutput, calls=%fused_computation.33 | convolution fusion | flops 805306368 | bytes 4980736 | tf_op jit(solution)/shard_map/secd,edf->secf/dot_general | solution.py:69
  81.6 1.9 fusion.45
  83.4 31.3 %all-to-all-done.1 = bf16[64,1,12,2048]{3,0,1,2:T(8,128)(2,1)} async-done(((bf16[64,1,12,2048]{3,0,1,2:T(8,128)(2,1)}), bf16[64,1,12,2048]{3,0,1,2:T(8,128)(2,1)}, u32[]{:S(2)}, u32[]{:S(2)}) %all-to-all-start.1) | async-done | bytes 3145760 | tf_op jit(solution)/shard_map/all_to_all | solution.py:66
  114.7 3.9 %multiply_convert_fusion.3 = (bf16[64,1,12,256]{3,0,2,1:T(8,128)(2,1)S(1)}, bf16[64,1,12,256]{3,0,2,1:T(8,128)(2,1)S(1)}) fusion(f32[64,1,12,256]{3,0,2,1:T(8,128)} %fusion.48, f32[64,1,12,256]{3,0,2,1:T(8,128)} %fusion.45, bf16[1,256,2048]{2,1,0:T(8,128)(2,1)} %param.18, bf16[64,1,12,2048]{3,0,1,2:T(8,128)(2,1)} %all-to-all-done.1), kind=kOutput, calls=%fused_computation.43 | convolution fusion | flops 807862272 | bytes 6553600 | tf_op jit(solution)/shard_map/secd,efd->secf/dot_general | solution.py:75
  118.7 1.0 fusion.51
  119.7 0.4 copy-done.3
  120.2 1.0 add_convert_fusion
  121.6 38.7 %all_to_all.26 = bf16[4,64,1,12,512]{4,1,3,2,0:T(8,128)(2,1)} all-to-all(bf16[4,64,1,12,512]{4,1,3,2,0:T(8,128)(2,1)S(1)} %bitcast.163), channel_id=1, replica_groups=mesh['sp'=64,'tp'=4] {'tp'}, dimensions={0} | all-to-all | bytes 6291456 | tf_op jit(solution)/shard_map/all_to_all | solution.py:15
  160.3 3.5 %reduce_sum.48 = bf16[64,12,512]{2,0,1:T(8,128)(2,1)} reduce(bf16[4,64,1,12,512]{4,1,3,2,0:T(8,128)(2,1)} %all_to_all.26, bf16[]{:T(256)} %constant.12.clone.1), dimensions={0,2}, to_apply=%region_4.5 | reduce | flops 1179648 | bytes 3932162 | tf_op jit(solution)/shard_map/reduce_sum | solution.py:16
  163.8 2.5 copy.54
  166.3 9.5 %all-to-all-start.3 = ((bf16[64,1,12,512]{3,2,1,0:T(8,128)(2,1)}), bf16[64,1,12,512]{3,2,1,0:T(8,128)(2,1)}, u32[]{:S(2)}, u32[]{:S(2)}) async-start(bf16[64,1,12,512]{3,2,1,0:T(8,128)(2,1)} %copy.54), calls=%async_computation.3 | async-start | bytes 2097152 | tf_op jit(solution)/shard_map/all_to_all | solution.py:94
  175.9 3.5 %collective-permute-start = (bf16[2,2,256]{2,1,0:T(2,128)(2,1)S(1)}, bf16[2,2,256]{2,1,0:T(2,128)(2,1)S(1)}, u32[]{:S(2)}, u32[]{:S(2)}) collective-permute-start(bf16[2,2,256]{2,1,0:T(2,128)(2,1)S(1)} %pad_maximum_fusion.2), channel_id=1, source_target_pairs={{0,4},{4,8},{8,12},{12,16},{16,20},{20,24},{24,28},{28,32},{32,36}... | collective-permute-start | bytes 6152 | tf_op jit(solution)/shard_map/ppermute | solution.py:22
  179.7 0.7 convert_multiply_fusion.1
  180.4 0.7 copy.51
  181.2 0.6 multiply_bitcast_fusion
  181.7 22.2 %all-to-all-done.3 = bf16[64,1,12,512]{3,2,1,0:T(8,128)(2,1)} async-done(((bf16[64,1,12,512]{3,2,1,0:T(8,128)(2,1)}), bf16[64,1,12,512]{3,2,1,0:T(8,128)(2,1)}, u32[]{:S(2)}, u32[]{:S(2)}) %all-to-all-start.3) | async-done | bytes 786464 | tf_op jit(solution)/shard_map/all_to_all | solution.py:94
  203.9 2.1 reshape.161
  206.0 3.3 %gather_fusion = bf16[384,512]{1,0:T(8,128)(2,1)S(1)} fusion(bf16[768,512]{1,0:T(8,128)(2,1)} %reshape.161, s32[1024]{0:T(1024)S(1)} %pad_clamp_fusion), kind=kCustom, calls=%fused_computation | custom fusion | bytes 787968 | tf_op jit(solution)/shard_map/jit(_take)/gather | solution.py:99
  209.3 0.9 gather.7
  210.2 2.2 convert_reduce_fusion.1
  212.4 1.0 add_convert_fusion.1
  213.4 11.0 %all_gather.3 = bf16[192,2048]{1,0:T(8,128)(2,1)S(1)} all-gather(bf16[192,512]{1,0:T(8,128)(2,1)S(1)} %add_convert_fusion.1), channel_id=1, replica_groups=mesh['sp'=64,'tp'=4] {'tp'}, dimensions={1}, use_global_device_ids=true | all-gather | bytes 983040 | tf_op jit(solution)/shard_map/all_gather | solution.py:106
  224.4 2.5 multiply_convert_fusion.6
  226.8 1.5 convolution_convert_fusion
  228.3 9.5 %all-to-all-start.4 = ((bf16[64,32,256]{2,1,0:T(8,128)(2,1)}), bf16[64,32,256]{2,1,0:T(8,128)(2,1)}, u32[]{:S(2)}, u32[]{:S(2)}) async-start(bf16[64,32,256]{2,1,0:T(8,128)(2,1)} %bitcast.167), calls=%async_computation.4 | async-start | bytes 2097152 | tf_op jit(solution)/shard_map/all_to_all | solution.py:15
  237.8 3.1 %fusion.33 = bf16[1,2048,256]{1,2,0:T(8,128)(2,1)} fusion(bf16[64,1,12,2048]{3,0,2,1:T(8,128)(2,1)S(1)} %copy-done, bf16[64,1,12,256]{3,0,2,1:T(8,128)(2,1)} %copy-done.12), kind=kOutput, calls=%fused_computation.25 | convolution fusion | flops 805830656 | bytes 4587520 | tf_op jit(solution)/shard_map/secd,secf->edf/dot_general | solution.py:81
  240.9 4.0 %fusion.30 = bf16[1,256,2048]{2,1,0:T(8,128)(2,1)} fusion(bf16[64,1,12,2048]{3,0,1,2:T(8,128)(2,1)} %all-to-all-done.1, f32[64,1,12,256]{3,0,2,1:T(8,128)S(1)} %copy-done.18, f32[64,1,12,256]{3,0,2,1:T(8,128)S(1)} %copy-done.17), kind=kOutput, calls=%fused_computation.24 | convolution fusion | flops 807010304 | bytes 5767168 | tf_op jit(solution)/shard_map/secf,secd->efd/dot_general | solution.py:78
  244.9 0.6 slice.66
  245.5 2.5 collective-permute-start.1
  248.1 2.0 fusion.36
  250.0 2.3 copy.55
  252.3 2.3 copy.56
  254.6 0.7 fusion.72
  255.3 0.7 fusion.71
  256.0 10.0 %all-to-all-done.4 = bf16[64,32,256]{2,1,0:T(8,128)(2,1)} async-done(((bf16[64,32,256]{2,1,0:T(8,128)(2,1)}), bf16[64,32,256]{2,1,0:T(8,128)(2,1)}, u32[]{:S(2)}, u32[]{:S(2)}) %all-to-all-start.4) | async-done | bytes 1048608 | tf_op jit(solution)/shard_map/all_to_all | solution.py:15
  266.0 2.0 convert_reduce_fusion
  (58 shorter events, 1.9 us)
Async XLA Ops:
  0.6 77.7 %copy-start = (bf16[64,1,12,2048]{3,0,2,1:T(8,128)(2,1)S(1)}, bf16[64,1,12,2048]{3,0,2,1:T(8,128)(2,1)}, u32[]{:S(2)}) copy-start(bf16[64,1,12,2048]{3,0,2,1:T(8,128)(2,1)} %param.15) | copy-start | bytes 9437188
  8.6 5.3 %copy-start.16 = (f32[192,2]{0,1:T(2,128)S(1)}, f32[192,2]{0,1:T(2,128)}, u32[]{:S(2)}) copy-start(f32[192,2]{0,1:T(2,128)} %param.14) | copy-start | bytes 4612
  73.5 41.2 %all-to-all-start.1 = ((bf16[64,1,12,2048]{3,0,1,2:T(8,128)(2,1)}), bf16[64,1,12,2048]{3,0,1,2:T(8,128)(2,1)}, u32[]{:S(2)}, u32[]{:S(2)}) async-start(bf16[64,1,12,2048]{3,0,1,2:T(8,128)(2,1)} %bitcast.164), calls=%async_computation.1 | async-start | bytes 6291456 | tf_op jit(solution)/shard_map/all_to_all | solution.py:66
  78.4 3.2 %copy-start.2 = (bf16[1,2048,256]{2,1,0:T(8,128)(2,1)S(1)}, bf16[1,2048,256]{2,1,0:T(8,128)(2,1)}, u32[]{:S(2)}) copy-start(bf16[1,2048,256]{2,1,0:T(8,128)(2,1)} %param.17) | copy-start | bytes 3145732
  114.7 3.9 %copy-start.1 = (bf16[1,2048,256]{2,1,0:T(8,128)(2,1)S(1)}, bf16[1,2048,256]{2,1,0:T(8,128)(2,1)}, u32[]{:S(2)}) copy-start(bf16[1,2048,256]{2,1,0:T(8,128)(2,1)} %param.16) | copy-start | bytes 3145732
  118.6 1.1 copy-start.12
  118.6 1.1 copy-start.10
  118.7 1.5 copy-start.3
  160.3 15.6 %copy-start.5 = (bf16[192,256]{1,0:T(8,128)(2,1)S(1)}, bf16[192,256]{1,0:T(8,128)(2,1)}, u32[]{:S(2)}) copy-start(bf16[192,256]{1,0:T(8,128)(2,1)} %param.19) | copy-start | bytes 294916
  160.3 15.6 %copy-start.7 = (bf16[192,256]{1,0:T(8,128)(2,1)S(1)}, bf16[192,256]{1,0:T(8,128)(2,1)}, u32[]{:S(2)}) copy-start(bf16[192,256]{1,0:T(8,128)(2,1)} %param.21) | copy-start | bytes 294916
  160.3 19.4 %copy-start.13 = (s32[192,2]{0,1:T(2,128)S(1)}, s32[192,2]{0,1:T(2,128)}, u32[]{:S(2)}) copy-start(s32[192,2]{0,1:T(2,128)} %param.13) | copy-start | bytes 4612
  160.3 19.4 %copy-start.15 = (f32[3,256]{1,0:T(4,128)S(1)}, f32[3,256]{1,0:T(4,128)}, u32[]{:S(2)}) copy-start(f32[3,256]{1,0:T(4,128)} %param.22) | copy-start | bytes 9220
  166.3 37.6 %all-to-all-start.3 = ((bf16[64,1,12,512]{3,2,1,0:T(8,128)(2,1)}), bf16[64,1,12,512]{3,2,1,0:T(8,128)(2,1)}, u32[]{:S(2)}, u32[]{:S(2)}) async-start(bf16[64,1,12,512]{3,2,1,0:T(8,128)(2,1)} %copy.54), calls=%async_computation.3 | async-start | bytes 2097152 | tf_op jit(solution)/shard_map/all_to_all | solution.py:94
  175.9 5.3 %collective-permute-start = (bf16[2,2,256]{2,1,0:T(2,128)(2,1)S(1)}, bf16[2,2,256]{2,1,0:T(2,128)(2,1)S(1)}, u32[]{:S(2)}, u32[]{:S(2)}) collective-permute-start(bf16[2,2,256]{2,1,0:T(2,128)(2,1)S(1)} %pad_maximum_fusion.2), channel_id=1, source_target_pairs={{0,4},{4,8},{8,12},{12,16},{16,20},{20,24},{24,28},{28,32},{32,36}... | collective-permute-start | bytes 6152 | tf_op jit(solution)/shard_map/ppermute | solution.py:22
  209.3 15.1 %copy-start.14 = (f32[2,256]{1,0:T(2,128)S(1)}, f32[2,256]{1,0:T(2,128)}, u32[]{:S(2)}) copy-start(f32[2,256]{1,0:T(2,128)} %multiply_bitcast_fusion) | copy-start | bytes 6148
  210.2 16.6 %copy-start.9 = (bf16[192,256]{1,0:T(8,128)(2,1)S(1)}, bf16[192,256]{1,0:T(8,128)(2,1)}, u32[]{:S(2)}) copy-start(bf16[192,256]{1,0:T(8,128)(2,1)} %param.20) | copy-start | bytes 294916
  213.4 14.9 %copy-start.4 = (bf16[192,512]{1,0:T(8,128)(2,1)}, bf16[192,512]{1,0:T(8,128)(2,1)S(1)}, u32[]{:S(2)}) copy-start(bf16[192,512]{1,0:T(8,128)(2,1)S(1)} %add_convert_fusion.1) | copy-start | bytes 589828
  228.3 37.7 %all-to-all-start.4 = ((bf16[64,32,256]{2,1,0:T(8,128)(2,1)}), bf16[64,32,256]{2,1,0:T(8,128)(2,1)}, u32[]{:S(2)}, u32[]{:S(2)}) async-start(bf16[64,32,256]{2,1,0:T(8,128)(2,1)} %bitcast.167), calls=%async_computation.4 | async-start | bytes 2097152 | tf_op jit(solution)/shard_map/all_to_all | solution.py:15
  237.8 3.1 %copy-start.17 = (f32[64,1,12,256]{3,0,2,1:T(8,128)S(1)}, f32[64,1,12,256]{3,0,2,1:T(8,128)}, u32[]{:S(2)}) copy-start(f32[64,1,12,256]{3,0,2,1:T(8,128)} %fusion.48) | copy-start | bytes 2359300
  237.8 3.1 %copy-start.18 = (f32[64,1,12,256]{3,0,2,1:T(8,128)S(1)}, f32[64,1,12,256]{3,0,2,1:T(8,128)}, u32[]{:S(2)}) copy-start(f32[64,1,12,256]{3,0,2,1:T(8,128)} %fusion.45) | copy-start | bytes 2359300
  240.9 7.1 %copy-start.11 = (bf16[64,1,12,256]{3,0,2,1:T(8,128)(2,1)S(1)}, bf16[64,1,12,256]{3,0,2,1:T(8,128)(2,1)}, u32[]{:S(2)}) copy-start(bf16[64,1,12,256]{3,0,2,1:T(8,128)(2,1)} %copy-done.10) | copy-start | bytes 1179652
  245.5 9.1 %collective-permute-start.1 = (f32[2,256]{1,0:T(2,128)}, f32[2,256]{1,0:T(2,128)S(1)}, u32[]{:S(2)}, u32[]{:S(2)}) collective-permute-start(f32[2,256]{1,0:T(2,128)} %slice.66), channel_id=1, source_target_pairs={{4,0},{8,4},{12,8},{16,12},{20,16},{24,20},{28,24},{32,28},{36,32}... | collective-permute-start | bytes 6152 | tf_op jit(solution)/shard_map/ppermute | solution.py:22
  250.0 4.6 %copy-start.6 = (bf16[192,256]{1,0:T(8,128)(2,1)S(1)}, bf16[192,256]{1,0:T(8,128)(2,1)}, u32[]{:S(2)}) copy-start(bf16[192,256]{1,0:T(8,128)(2,1)} %param.19) | copy-start | bytes 294916
  250.0 5.3 %copy-start.8 = (bf16[192,256]{1,0:T(8,128)(2,1)S(1)}, bf16[192,256]{1,0:T(8,128)(2,1)}, u32[]{:S(2)}) copy-start(bf16[192,256]{1,0:T(8,128)(2,1)} %param.21) | copy-start | bytes 294916
